TPU v7x, 128 devices: a whole 4x4x4 slice. The times are simulated.
128 devices in a mesh: sp: 16 (over z, y), tp: 8 (over x, core).
Axes of the slice: x: 4, y: 4, z: 4, core: 2. Of those that a mesh axis runs over, the one named last changes fastest.
Arguments:
- hidden_activations: bfloat16 [12288, 4096], P(('sp', 'tp')), may hold values from -6 to 6
- entry_rescale_vector: bfloat16 [4096], replicated, may hold values from 0.099609375 to 1.8984375
- probe_matrix: bfloat16 [4096, 2048], P('sp', 'tp'), may hold values from -0.09375 to 0.09375
- lookup_address_matrix: bfloat16 [4096, 2048], P('sp', 'tp'), may hold values from -0.09375 to 0.09375
- payload_matrix: bfloat16 [4096, 4096], P('sp', 'tp'), may hold values from -0.09375 to 0.09375
- postfilter_switch_matrix: bfloat16 [4096, 4096], P('sp', 'tp'), may hold values from -0.09375 to 0.09375
- prefilter_switch_matrix: bfloat16 [4096, 4096], P('sp', 'tp'), may hold values from -0.09375 to 0.09375
- filter_source_matrix: bfloat16 [4096, 4096], P('sp', 'tp'), may hold values from -0.09375 to 0.09375
- forget_left_factor: bfloat16 [4096, 64], replicated, may hold values from -0.09375 to 0.09375
- forget_right_factor: bfloat16 [64, 2048], P(None, 'tp'), may hold values from -0.75 to 0.75
- forget_offset_per_feature: float32 [2048], P('tp'), may hold values from -1 to 12
- forget_spike_additions: float32 [16, 12288], P('tp', 'sp'), may hold values from -3 to 0
- subspace_rescale_vector: bfloat16 [16, 256], P('tp'), may hold values from 0.099609375 to 1.8984375
- depthwise_filter_taps: bfloat16 [3, 4096], P(None, 'tp'), may hold values from -3.5 to 3.5
- mixer_result_matrix: bfloat16 [4096, 4096], P('tp'), may hold values from -0.09375 to 0.09375
- filter_result_matrix: bfloat16 [4096, 4096], P('tp'), may hold values from -0.09375 to 0.09375
Outputs:
- mixed: bfloat16 [12288, 4096], P(('sp', 'tp'))
All inputs are finite; a program needn't handle non-finite values.
Results may differ from a plain program's by a relative error of at most 0.02.
Values may be sent and summed in bfloat16 or wider, within the bound.
No kernel may reach another device: no remote copies, remote signals or barrier semaphores. Data moves between devices by JAX's collectives and lax.ppermute only.
A program may use at most 128 MiB of HBM per device.

v0:
```python
import jax
import jax.numpy as jnp
from jax import lax
from jax.sharding import Mesh
from jax.sharding import PartitionSpec as P

BLOCK = 64
SP = ("sp_0", "sp_1")
SP_TP = ("sp_0", "sp_1", "tp")
epsilon = 1e-06
softness_scale = 16.0


def nothing_yet(shard, identity):
    return jax.tree.map(
        lambda part, zero: jnp.zeros_like(part) + jnp.asarray(zero, part.dtype), shard, identity
    )


def entering(shard, axes, combine, identity):
    before = start = nothing_yet(shard, identity)
    total = shard
    for axis in reversed(axes):
        size, index = (lax.axis_size(axis), lax.axis_index(axis))
        pieces = jax.tree.map(
            lambda part, kind: lax.all_gather(part.astype(kind), axis),
            total,
            (jnp.bfloat16, jnp.bfloat16),
        )
        inside, total = (start, start)
        for k in range(size):
            passed = k < index
            total = combine(
                total, jax.tree.map(lambda part, own: part[k].astype(own.dtype), pieces, shard)
            )
            inside = jax.tree.map(lambda new, old: jnp.where(passed, new, old), total, inside)
        before = combine(inside, before)
    return before


def shifted(value, axis, steps):
    count = lax.axis_size(axis)
    leading, last = (max(0, -steps), min(count, count - steps))
    return lax.ppermute(value, axis, [(source, source + steps) for source in range(leading, last)])


def in_one_piece(arrays, axis, dim, along):
    both = jnp.concatenate(arrays, axis=along)
    out, at, gathered = (lax.all_gather(both, axis, axis=dim, tiled=True), 0, [])
    for a in arrays:
        gathered.append(lax.slice_in_dim(out, at, at + a.shape[along], axis=along))
        at += a.shape[along]
    return tuple(gathered)


def norm_values(rows, gain):
    rows_f = rows.astype(jnp.float32)
    meansq = jnp.mean(rows_f * rows_f, axis=-1, keepdims=True)
    return rows_f * lax.rsqrt(meansq + epsilon) * gain.astype(jnp.float32)


def row_norm(gain, rows):
    return norm_values(rows, gain).astype(jnp.bfloat16)


def project_rows(normalized_input):

    def accumulate(totals, weight_rows, offset):
        return tuple(
            (
                jnp.dot(normalized_input, rows_now, preferred_element_type=jnp.float32)
                for rows_now in weight_rows
            )
        )

    return accumulate


def empty_slots(normalized_input, weight_list):
    return tuple(
        (
            jnp.zeros((normalized_input.shape[0], weight.shape[1]), jnp.float32)
            for weight in weight_list
        )
    )


def block_terms(query_rows, key_rows, value_rows, forget_log_rate):
    length_value, head_number, key_dim = query_rows.shape
    value_dim = value_rows.shape[2]
    block_count = length_value // BLOCK
    key_shape = (block_count, BLOCK, head_number, key_dim)
    query_f32 = query_rows.astype(jnp.float32).reshape(key_shape) * key_dim ** (-0.5)
    key_f32 = key_rows.astype(jnp.float32).reshape(key_shape)
    value_f32 = value_rows.astype(jnp.float32).reshape(block_count, BLOCK, head_number, value_dim)
    within = jnp.cumsum(forget_log_rate.reshape(key_shape), axis=1)
    block_end = within[:, -1]
    query_decayed = query_f32 * jnp.exp(within)
    key_inverse = key_f32 * jnp.exp(-within)
    key_tail = key_f32 * jnp.exp(block_end[:, None] - within)
    highest = lax.Precision.HIGHEST
    scores = jnp.einsum("nihd,njhd->nhij", query_decayed, key_inverse, precision=highest)
    causal = jnp.tril(jnp.ones((BLOCK, BLOCK), dtype=bool))
    scores = jnp.where(causal, scores, 0.0)
    inside = jnp.einsum("nhij,njhv->nihv", scores, value_f32, precision=highest)
    updates = jnp.einsum("njhd,njhv->nhdv", key_tail, value_f32, precision=highest)

    def advance(state, pair):
        decay_now, update_now = pair
        return (jnp.exp(decay_now)[..., None] * state + update_now, state)

    start_state = jnp.zeros((head_number, key_dim, value_dim), jnp.float32)
    final_state, state_in = lax.scan(advance, start_state, (block_end, updates))
    carried = jnp.einsum("nihd,nhdv->nihv", query_decayed, state_in, precision=highest)
    return (inside + carried, query_decayed, block_end, final_state)


def chain_combine(earlier, later):
    return (earlier[0] * later[0], later[0][..., None] * earlier[1] + later[1])


def attention_path(
    normalized_input,
    sum_values,
    forget_left_factor,
    forget_right_factor,
    forget_offset_per_feature,
    forget_spike_additions,
    subspace_rescale_vector,
):
    length_value = normalized_input.shape[0]
    head_number = subspace_rescale_vector.shape[0]
    value_dim = subspace_rescale_vector.shape[1]
    query_rows = sum_values[0].astype(jnp.bfloat16).reshape(length_value, head_number, -1)
    key_rows = sum_values[1].astype(jnp.bfloat16).reshape(length_value, head_number, -1)
    value_rows = sum_values[2].astype(jnp.bfloat16).reshape(length_value, head_number, value_dim)
    low_rank = jnp.dot(
        normalized_input, forget_left_factor, preferred_element_type=jnp.float32
    ).astype(jnp.bfloat16)
    gate_preactivation = (
        jnp.dot(low_rank, forget_right_factor, preferred_element_type=jnp.float32)
        + forget_offset_per_feature
    )
    forget_log_rate = (jax.nn.log_sigmoid(gate_preactivation) / softness_scale).reshape(
        length_value, head_number, -1
    )
    forget_log_rate = forget_log_rate + jnp.transpose(forget_spike_additions)[:, :, None]
    local_out, query_decayed, block_end, final_state = block_terms(
        query_rows, key_rows, value_rows, forget_log_rate
    )
    prefix = jnp.cumsum(block_end, axis=0) - block_end
    query_far = query_decayed * jnp.exp(prefix)[:, None]
    total_decay = jnp.exp(jnp.sum(block_end, axis=0))
    identity = (jnp.ones_like(total_decay), jnp.zeros_like(final_state))
    incoming = entering((total_decay, final_state), SP, chain_combine, identity)[1]
    attended = local_out + jnp.einsum(
        "nihd,hdv->nihv", query_far, incoming, precision=lax.Precision.HIGHEST
    )
    attended = attended.reshape(length_value, head_number, value_dim)
    return (
        norm_values(attended, subspace_rescale_vector)
        .astype(jnp.bfloat16)
        .reshape(length_value, head_number * value_dim)
    )


def conv_branch(sum_values, depthwise_filter_taps):
    outer = sum_values[0].astype(jnp.bfloat16)
    inner = sum_values[1].astype(jnp.bfloat16)
    conv_in = sum_values[2].astype(jnp.bfloat16)
    length_value = outer.shape[0]
    gated_in = (inner.astype(jnp.float32) * conv_in.astype(jnp.float32)).astype(jnp.bfloat16)
    reach = depthwise_filter_taps.shape[0] - 1
    rim_rows = shifted(gated_in[length_value - reach :], SP, 1)
    padded = jnp.concatenate([rim_rows, gated_in], axis=0)
    taps_f32 = depthwise_filter_taps.astype(jnp.float32)
    conv_sum = jnp.zeros(outer.shape, jnp.float32)
    for tap_index in range(depthwise_filter_taps.shape[0]):
        conv_sum = conv_sum + taps_f32[tap_index] * padded[
            tap_index : tap_index + length_value
        ].astype(jnp.float32)
    return (conv_sum * outer.astype(jnp.float32)).astype(jnp.bfloat16)


def body(
    hidden_activations,
    entry_rescale_vector,
    probe_matrix,
    lookup_address_matrix,
    payload_matrix,
    postfilter_switch_matrix,
    prefilter_switch_matrix,
    filter_source_matrix,
    forget_left_factor,
    forget_right_factor,
    forget_offset_per_feature,
    forget_spike_additions,
    subspace_rescale_vector,
    depthwise_filter_taps,
    mixer_result_matrix,
    filter_result_matrix,
):
    normalized_input = row_norm(
        entry_rescale_vector, lax.all_gather(hidden_activations, "tp", axis=0, tiled=True)
    )
    accumulate = project_rows(normalized_input)
    attn_sums = accumulate(
        empty_slots(normalized_input, (probe_matrix, lookup_address_matrix, payload_matrix)),
        in_one_piece((probe_matrix, lookup_address_matrix, payload_matrix), SP, 0, 1),
        jnp.int32(0),
    )
    mixed_attn = attention_path(
        normalized_input,
        attn_sums,
        forget_left_factor,
        forget_right_factor,
        forget_offset_per_feature,
        forget_spike_additions,
        subspace_rescale_vector,
    )
    conv_sums = accumulate(
        empty_slots(
            normalized_input,
            (postfilter_switch_matrix, prefilter_switch_matrix, filter_source_matrix),
        ),
        in_one_piece(
            (postfilter_switch_matrix, prefilter_switch_matrix, filter_source_matrix), SP, 0, 1
        ),
        jnp.int32(0),
    )
    mixed_conv = conv_branch(conv_sums, depthwise_filter_taps)
    return lax.psum_scatter(
        (
            jnp.dot(mixed_attn, mixer_result_matrix, preferred_element_type=jnp.float32)
            + jnp.dot(mixed_conv, filter_result_matrix, preferred_element_type=jnp.float32)
        ).astype(jnp.bfloat16),
        "tp",
        scatter_dimension=0,
        tiled=True,
    )


def solution(mesh):
    split = Mesh(mesh.devices.reshape(4, 4, mesh.shape["tp"]), ("sp_0", "sp_1", "tp"))
    in_specs = (
        P(SP_TP, None),
        P(),
        P(SP, "tp"),
        P(SP, "tp"),
        P(SP, "tp"),
        P(SP, "tp"),
        P(SP, "tp"),
        P(SP, "tp"),
        P(),
        P(None, "tp"),
        P("tp"),
        P("tp", SP),
        P("tp", None),
        P(None, "tp"),
        P("tp", None),
        P("tp", None),
    )
    out_specs = P(SP_TP, None)
    return jax.shard_map(body, mesh=split, in_specs=in_specs, out_specs=out_specs, check_vma=False)
```

profile of v0, /device:TPU:1, one launch (start us, length us, event | category | flops | bytes accessed | tf_op | source)
XLA Modules:
  0.0 311.4 jit_solution(12454789588959216576)
XLA Ops:
  7.3 1.9 pad_maximum_fusion.3
  9.3 2.1 pad_maximum_fusion.2
  11.8 41.7 %all-gather.7.cloned.1.call-done = bf16[768,4096]{1,0:T(8,128)(2,1)} async-done(((bf16[96,4096]{1,0:T(8,128)(2,1)}), bf16[768,4096]{1,0:T(8,128)(2,1)}) %all-gather.7.cloned.1.call-update) | async-done | bytes 6291472 | tf_op jit(solution)/shard_map/all_gather | solution.py:204
  53.5 4.2 %fusion = f32[768]{0:T(1024)S(1)} fusion(bf16[768,4096]{1,0:T(8,128)(2,1)} %all-gather.7.cloned.1.call-done), kind=kLoop, calls=%fused_computation.6 | loop fusion | flops 9436416 | bytes 6294528 | tf_op jit(solution)/shard_map/reduce_sum | solution.py:58
  58.1 5.4 %fusion.2 = bf16[768,4096]{1,0:T(8,128)(2,1)} fusion(bf16[768,4096]{1,0:T(8,128)(2,1)S(1)} %copy-done.2, f32[4096]{0:T(1024)S(1)} %convert_element_type.265, f32[768]{0:T(1024)S(1)} %add_rsqrt_fusion.1), kind=kLoop, calls=%fused_computation.8 | loop fusion | flops 12582912 | bytes 12602368 | tf_op jit(solution)/shard_map/convert_element_type | solution.py:63
  63.5 5.7 %fusion.49 = f32[768,256]{1,0:T(8,128)S(1)} fusion(bf16[64,256]{1,0:T(8,128)(2,1)S(1)} %copy-done.13, bf16[768,4096]{1,0:T(8,128)(2,1)} %fusion.2, bf16[4096,64]{0,1:T(8,128)(2,1)S(1)} %copy-done, f32[256]{0:T(256)S(1)} %copy-done.14), kind=kOutput, calls=%fused_computation.51 | convolution fusion | flops 429834240 | bytes 7635968 | tf_op jit(solution)/shard_map/dot_general | solution.py:141
  70.5 8.2 %all-gather.2 = bf16[4,2,128]{2,1,0:T(2,128)(2,1)S(1)} all-gather(bf16[1,2,128]{2,1,0:T(2,128)(2,1)S(1)} %fusion.121), channel_id=2, replica_groups=mesh['sp_0'=4,'sp_1'=4,'tp'=8] {'sp_1'}, dimensions={0}, use_global_device_ids=true | all-gather | bytes 2560 | tf_op jit(solution)/shard_map/all_gather | solution.py:26
  78.7 8.3 %all_gather.30 = bf16[4,2,128]{2,1,0:T(2,128)(2,1)S(1)} all-gather(bf16[1,2,128]{2,1,0:T(2,128)(2,1)S(1)} %get-tuple-element.96), channel_id=1, replica_groups=mesh['sp_0'=4,'sp_1'=4,'tp'=8] {'sp_0'}, dimensions={0}, use_global_device_ids=true | all-gather | bytes 2560 | tf_op jit(solution)/shard_map/all_gather | solution.py:26
  87.0 39.1 %all-gather.9.cloned.1.call-done = bf16[4096,1024]{1,0:T(8,128)(2,1)} async-done(((bf16[256,1024]{1,0:T(8,128)(2,1)}), bf16[4096,1024]{1,0:T(8,128)(2,1)}) %all-gather.9.cloned.1.call-update) | async-done | bytes 8388624 | tf_op jit(solution)/shard_map/all_gather | solution.py:49
  126.1 5.2 %fusion.42 = f32[768,256]{1,0:T(8,128)S(1)} fusion(bf16[768,4096]{1,0:T(8,128)(2,1)} %fusion.2, bf16[4096,1024]{1,0:T(8,128)(2,1)} %all-gather.9.cloned.1.call-done), kind=kOutput, calls=%fused_computation.39 | convolution fusion | flops 1611005952 | bytes 9175040 | tf_op jit(solution)/shard_map/dot_general | solution.py:71
  131.7 7.4 %fusion.15 = bf16[768,512]{1,0:T(8,128)(2,1)S(1)} fusion(bf16[768,4096]{1,0:T(8,128)(2,1)} %fusion.2, bf16[4096,1024]{1,0:T(8,128)(2,1)} %all-gather.9.cloned.1.call-done), kind=kOutput, calls=%fused_computation.28 | convolution fusion | flops 3221618688 | bytes 11272192 | tf_op jit(solution)/shard_map/dot_general | solution.py:71
  139.4 5.4 %fusion.36 = f32[768,256]{1,0:T(8,128)S(1)} fusion(bf16[768,4096]{1,0:T(8,128)(2,1)} %fusion.2, bf16[4096,1024]{1,0:T(8,128)(2,1)} %all-gather.9.cloned.1.call-done), kind=kOutput, calls=%fused_computation.37 | convolution fusion | flops 1611202560 | bytes 9175040 | tf_op jit(solution)/shard_map/dot_general | solution.py:71
  144.7 1.3 mul.250
  146.0 3.9 %copy_multiply_fusion = (f32[12,64,2,128]{3,0,1,2:T(8,128)S(1)}, f32[12,64,2,128]{3,0,1,2:T(8,128)}, f32[12,64,2,128]{3,0,1,2:T(8,128)}, f32[12,64,2,128]{3,0,1,2:T(8,128)S(1)}) fusion(f32[12,64,2,128]{3,2,1,0:T(2,128)S(1)} %reshape.177, f32[12,64,2,128]{3,0,1,2:T(8,128)} %copy-done.5, f32[12,2,128]{2,0,1:T(8,128)S(1)} %get-tuple-element.140, ...), kind=kLoop, calls=%fused_computation.41 | loop fusion | flops 1179648 | bytes 5529600 | tf_op jit(solution)/shard_map/mul | solution.py:100
  149.9 3.2 %fusion.52 = f32[12,2,128,256]{3,2,1,0:T(8,128)} fusion(f32[12,64,2,128]{3,0,1,2:T(8,128)S(1)} %get-tuple-element.85, bf16[12,64,2,256]{3,2,1,0:T(2,128)(2,1)S(1)} %reshape.174), kind=kOutput, calls=%fused_computation.56 | convolution fusion | flops 603979776 | bytes 4718592 | tf_op jit(solution)/shard_map/njhd,njhv->nhdv/dot_general | solution.py:106
  153.1 22.3 %while.13 = (s32[]{:T(128)}, f32[2,128,256]{2,1,0:T(8,128)S(1)}, f32[12,2,128,256]{3,2,1,0:T(8,128)}, f32[12,2,128]{2,0,1:T(8,128)S(1)}, f32[12,2,128,256]{3,2,1,0:T(8,128)}, /*index=5*/s32[]{:T(128)}, s32[]{:T(128)}) while((s32[]{:T(128)}, f32[2,128,256]{2,1,0:T(8,128)S(1)}, f32[12,2,128,256]{3,2,1,0:T(8,128)}, ...), condition=%wide.region_3.4_spmd.clone, body=%wide.region_2.3_spmd.clone.sunk | while | flops 262147 | bytes 1315948 | solution.py:113
  153.8 1.1 bitcast_add_fusion.3
  155.7 1.1 bitcast_add_fusion.3
  156.8 0.7 bitcast_dynamic-update-slice_fusion.2
  157.5 1.1 bitcast_add_fusion.3
  159.4 1.1 bitcast_add_fusion.3
  161.2 1.1 bitcast_add_fusion.3
  163.1 1.1 bitcast_add_fusion.3
  164.9 1.1 bitcast_add_fusion.3
  166.1 0.7 bitcast_dynamic-update-slice_fusion.2
  166.8 1.1 bitcast_add_fusion.3
  168.7 1.1 bitcast_add_fusion.3
  170.5 1.1 bitcast_add_fusion.3
  171.6 0.7 bitcast_dynamic-update-slice_fusion.2
  172.4 1.1 bitcast_add_fusion.3
  173.5 0.7 bitcast_dynamic-update-slice_fusion.2
  174.2 1.1 bitcast_add_fusion.3
  175.4 14.8 %all-gather.1 = bf16[8,128,256]{2,1,0:T(8,128)(2,1)S(1)} all-gather(bf16[2,128,256]{2,1,0:T(8,128)(2,1)S(1)} %convert_element_type.296), channel_id=3, replica_groups=mesh['sp_0'=4,'sp_1'=4,'tp'=8] {'sp_1'}, dimensions={0}, use_global_device_ids=true | all-gather | bytes 655360 | tf_op jit(solution)/shard_map/all_gather | solution.py:26
  190.4 14.6 %all_gather.33 = bf16[4,2,128,256]{3,2,1,0:T(8,128)(2,1)S(1)} all-gather(bf16[1,2,128,256]{3,2,1,0:T(8,128)(2,1)S(1)} %fusion.81), channel_id=1, replica_groups=mesh['sp_0'=4,'sp_1'=4,'tp'=8] {'sp_0'}, dimensions={0}, use_global_device_ids=true | all-gather | bytes 655360 | tf_op jit(solution)/shard_map/all_gather | solution.py:26
  205.0 3.1 convolution_select_fusion
  208.1 0.8 fusion.60
  208.9 2.1 fusion.62
  211.0 3.4 %multiply_reduce_fusion = (f32[12,64,2]{1,2,0:T(2,128)S(1)}, f32[12,64,2,256]{3,1,2,0:T(8,128)}) fusion(f32[12,64,2,128]{3,0,1,2:T(8,128)S(1)} %copy-done.7, bf16[4,2,128,256]{3,2,1,0:T(8,128)(2,1)S(1)} %all_gather.33, f32[2,128]{1,0:T(2,128)S(1)} %get-tuple-element.97, f32[2,128]{1,0:T(2,128)S(1)} %get-tuple-element.103, ...), kind=kOutput, calls=%fused_computation.27 | convolution fusion | flops 607648256 | bytes 6568968 | tf_op jit(solution)/shard_map/nihd,hdv->nihv/dot_general | solution.py:156
  214.6 1.2 mul.290
  216.0 1.2 copy.69
  217.2 1.3 copy.75
  218.5 3.5 %all-gather.11.cloned.1.call-done = bf16[4096,1536]{1,0:T(8,128)(2,1)} async-done(((bf16[256,1536]{1,0:T(8,128)(2,1)}), bf16[4096,1536]{1,0:T(8,128)(2,1)}) %all-gather.11.cloned.1.call-update) | async-done | bytes 12582928 | tf_op jit(solution)/shard_map/all_gather | solution.py:49
  222.0 7.4 %fusion.18 = bf16[768,512]{1,0:T(8,128)(2,1)S(1)} fusion(bf16[768,4096]{1,0:T(8,128)(2,1)} %fusion.2, bf16[4096,1536]{1,0:T(8,128)(2,1)} %all-gather.11.cloned.1.call-done), kind=kOutput, calls=%fused_computation.29 | convolution fusion | flops 3221618688 | bytes 11272192 | tf_op jit(solution)/shard_map/dot_general | solution.py:71
  229.4 7.6 %multiply_convert_fusion.1 = bf16[768,512]{1,0:T(8,128)(2,1)S(1)} fusion(bf16[768,512]{1,0:T(8,128)(2,1)S(1)} %fusion.18, bf16[768,4096]{1,0:T(8,128)(2,1)} %fusion.2, bf16[4096,1536]{1,0:T(8,128)(2,1)} %all-gather.11.cloned.1.call-done), kind=kOutput, calls=%fused_computation.25 | convolution fusion | flops 3223191552 | bytes 12058624 | tf_op jit(solution)/shard_map/dot_general | solution.py:71
  237.0 3.1 collective-permute-start
  240.2 6.4 %fusion.47 = f32[768,4096]{1,0:T(8,128)} fusion(bf16[512,4096]{1,0:T(8,128)(2,1)S(1)} %copy-done.6, f32[768,512]{1,0:T(8,128)S(1)} %bitcast.180, f32[768,512]{1,0:T(8,128)S(1)} %bitcast.179, f32[512]{0:T(512)S(1)} %bitcast.185), kind=kOutput, calls=%fused_computation.49 | convolution fusion | flops 3222405120 | bytes 19924992 | tf_op jit(solution)/shard_map/dot_general | solution.py:234
  246.6 15.3 %add_convert_fusion = bf16[768,4096]{1,0:T(8,128)(2,1)} fusion(f32[768,4096]{1,0:T(8,128)} %fusion.47, bf16[512,4096]{1,0:T(8,128)(2,1)} %param.33, bf16[768,512]{1,0:T(8,128)(2,1)S(1)} %multiply_convert_fusion.1, bf16[2,512]{1,0:T(2,128)(2,1)S(1)} %collective-permute-done, f32[512]{0:T(512)S(1)} %bitcast.189, f32[512]{0:T(512)S(1)} %bitcast.188, ...), kind=kOutput, calls=%fused_computation.9 | convolution fusion | flops 6455820288 | bytes 34349056 | tf_op jit(solution)/shard_map/dot_general | solution.py:235
  261.9 43.0 %reduce-scatter.2.cloned.1.call-done = bf16[96,4096]{1,0:T(8,128)(2,1)} async-done(((bf16[768,4096]{1,0:T(8,128)(2,1)}), bf16[96,4096]{1,0:T(8,128)(2,1)}) %reduce-scatter.2.cloned.1.call-update) | async-done | bytes 786448 | tf_op jit(solution)/shard_map/reduce_scatter | solution.py:232
  (99 shorter events, 9.9 us)
Async XLA Ops:
  6.5 57.0 %copy-start = (bf16[4096,64]{0,1:T(8,128)(2,1)S(1)}, bf16[4096,64]{0,1:T(8,128)(2,1)}, u32[]{:S(2)}) copy-start(bf16[4096,64]{0,1:T(8,128)(2,1)} %param.26) | copy-start | bytes 1572868
  6.5 4.9 %copy-start.12 = (bf16[2,256]{1,0:T(2,128)(2,1)S(1)}, bf16[2,256]{1,0:T(2,128)(2,1)}, u32[]{:S(2)}) copy-start(bf16[2,256]{1,0:T(2,128)(2,1)} %param.30) | copy-start | bytes 3076
  6.5 5.0 %copy-start.10 = (bf16[4096]{0:T(1024)(128)(2,1)S(1)}, bf16[4096]{0:T(1024)(128)(2,1)}, u32[]{:S(2)}) copy-start(bf16[4096]{0:T(1024)(128)(2,1)} %param.19) | copy-start | bytes 24580
  6.5 5.0 %copy-start.11 = (f32[2,768]{1,0:T(2,128)S(1)}, f32[2,768]{1,0:T(2,128)}, u32[]{:S(2)}) copy-start(f32[2,768]{1,0:T(2,128)} %param.29) | copy-start | bytes 18436
  6.5 5.2 %copy-start.9 = (bf16[3,512]{1,0:T(4,128)(2,1)S(1)}, bf16[3,512]{1,0:T(4,128)(2,1)}, u32[]{:S(2)}) copy-start(bf16[3,512]{1,0:T(4,128)(2,1)} %param.31) | copy-start | bytes 9220
  6.5 46.9 %all-gather.7.cloned.1.call-start = ((), (), s32[]{:S(2)}) async-start(), calls=%async_computation.1 | async-start | bytes 7077888 | tf_op jit(solution)/shard_map/all_gather | solution.py:204
  7.3 118.8 %all-gather.9.cloned.1.call-start = ((), (), s32[]{:S(2)}) async-start(), calls=%async_computation.2 | async-start | bytes 8912896 | tf_op jit(solution)/shard_map/all_gather | solution.py:49
  9.2 212.8 %all-gather.11.cloned.1.call-start = ((), (), s32[]{:S(2)}) async-start(), calls=%async_computation.3 | async-start | bytes 13369344 | tf_op jit(solution)/shard_map/all_gather | solution.py:49
  11.4 293.5 %reduce-scatter.2.cloned.1.call-start = ((), (), s32[]{:S(2)}) async-start(), calls=%async_computation.4 | async-start | bytes 7077888 | tf_op jit(solution)/shard_map/reduce_scatter | solution.py:232
  53.5 4.6 %copy-start.2 = (bf16[768,4096]{1,0:T(8,128)(2,1)S(1)}, bf16[768,4096]{1,0:T(8,128)(2,1)}, u32[]{:S(2)}) copy-start(bf16[768,4096]{1,0:T(8,128)(2,1)} %all-gather.7.cloned.1.call-done) | copy-start | bytes 18874372
  58.1 5.4 %copy-start.13 = (bf16[64,256]{1,0:T(8,128)(2,1)S(1)}, bf16[64,256]{1,0:T(8,128)(2,1)}, u32[]{:S(2)}) copy-start(bf16[64,256]{1,0:T(8,128)(2,1)} %param.27) | copy-start | bytes 98308
  58.1 5.4 %copy-start.14 = (f32[256]{0:T(256)S(1)}, f32[256]{0:T(256)}, u32[]{:S(2)}) copy-start(f32[256]{0:T(256)} %param.28) | copy-start | bytes 3076
  70.4 60.9 %copy-start.5 = (f32[12,64,2,128]{3,0,1,2:T(8,128)}, f32[12,64,2,128]{3,0,1,2:T(8,128)S(1)}, u32[]{:S(2)}) copy-start(f32[12,64,2,128]{3,0,1,2:T(8,128)S(1)} %fusion.45) | copy-start | bytes 2359300
  175.3 33.6 %copy-start.8 = (f32[12,2,128,256]{3,2,1,0:T(8,128)S(1)}, f32[12,2,128,256]{3,2,1,0:T(8,128)}, u32[]{:S(2)}) copy-start(f32[12,2,128,256]{3,2,1,0:T(8,128)} %get-tuple-element.33) | copy-start | bytes 9437188
  208.1 2.9 copy-start.7
  214.6 1.4 copy-start.4
  229.4 10.7 %copy-start.3 = (f32[96,8,2,256]{3,1,2,0:T(8,128)S(1)}, f32[96,8,2,256]{3,1,2,0:T(8,128)}, u32[]{:S(2)}) copy-start(f32[96,8,2,256]{3,1,2,0:T(8,128)} %copy.75) | copy-start | bytes 4718596
  229.4 10.7 %copy-start.6 = (bf16[512,4096]{1,0:T(8,128)(2,1)S(1)}, bf16[512,4096]{1,0:T(8,128)(2,1)}, u32[]{:S(2)}) copy-start(bf16[512,4096]{1,0:T(8,128)(2,1)} %param.32) | copy-start | bytes 12582916
  237.0 9.5 %collective-permute-start = (bf16[2,512]{1,0:T(2,128)(2,1)S(1)}, bf16[2,512]{1,0:T(2,128)(2,1)S(1)}, u32[]{:S(2)}, u32[]{:S(2)}) collective-permute-start(bf16[2,512]{1,0:T(2,128)(2,1)S(1)} %slice.151), channel_id=1, source_target_pairs={{0,8},{8,16},{16,24},{24,32},{32,40},{40,48},{48,56},{56,64},{64,7... | collective-permute-start | bytes 6152 | tf_op jit(solution)/shard_map/ppermute | solution.py:44
  246.6 58.4 %copy-start.1 = (bf16[4096,64]{0,1:T(8,128)(2,1)S(1)}, bf16[4096,64]{0,1:T(8,128)(2,1)}, u32[]{:S(2)}) copy-start(bf16[4096,64]{0,1:T(8,128)(2,1)} %param.26) | copy-start | bytes 1572868
Sparse Core Ops, SparseCore 0:
  9.0 44.4 all-gather.6
  55.6 70.4 all-gather.8
  128.3 93.7 all-gather.10
  262.0 42.8 reduce-scatter.1
where the time goes:
time: 312 us; the launch traced here: 311 us
  waiting for transfers between devices  128 us (41%)
  matrix products  72.9 us (23%)
  blocking collectives  45.9 us (15%)
  other arithmetic  40.2 us (13%)
  between operations  13.5 us (4%)
  local copies, waits for them, and re-layouts  7.15 us (2%)
  starting transfers between devices  3.27 us (1%)
    all_gather x4, blocking collectives, entering(): lax.all_gather(part.astype(kind), axis)  45.9 us
    reduce_scatter x1, waiting for transfers between devices, body(): lax.psum_scatter((jnp.dot(mixed_attn, mixer_result_matrix, preferred_elem...  43 us
    all_gather x2, waiting for transfers between devices, in_one_piece(): lax.all_gather(both, axis, axis=dim, tiled=True)  42.6 us
    all_gather x1, waiting for transfers between devices, body(): lax.all_gather(hidden_activations, 'tp', axis=0, tiled=True)  41.7 us
    dot_general x5, matrix products, accumulate(): jnp.dot(normalized_input, rows_now, preferred_element_type=jnp.float32)  32.9 us
    dot_general x1, matrix products, body(): jnp.dot(mixed_conv, filter_result_matrix, preferred_element_type=jnp.floa...  15.3 us
    add x12, other arithmetic, advance(): return (jnp.exp(decay_now)[..., None] * state + update_now, state)  12.9 us
    dynamic_update_slice x12, other arithmetic, block_terms(): final_state, state_in = lax.scan(advance, start_state, (block_end, updates))  8.77 us
  transfers between devices with their start and end apart: 5, of which 4 were waited for; matrix products, arithmetic and copies ran while one was open for 29% of the time, Pallas kernels for 0%

commit v1 on v0

--- a/solution.py
+++ b/solution.py
@@ -9,6 +9,28 @@
 SP_TP = ("sp_0", "sp_1", "tp")
 epsilon = 1e-06
 softness_scale = 16.0
+
+
+def joined_along(parts, dim):
+    lengths = list(parts.shape[1:])
+    lengths[dim] *= parts.shape[0]
+    return jnp.moveaxis(parts, 0, dim).reshape(lengths)
+
+
+def collect(array, axis, dim):
+    size = lax.axis_size(axis)
+    pairs = [(i, (i + 1) % size) for i in range(size)]
+    back = [(b, a) for a, b in pairs]
+    lower, upper = ([], [])
+    for step in range(size - 1):
+        if step % 2 == 0:
+            lower.append(lax.ppermute(lower[-1] if lower else array, axis, pairs))
+        else:
+            upper.append(lax.ppermute(upper[-1] if upper else array, axis, back))
+    tiles = jnp.stack([*lower[::-1], array, *upper])
+    shift = lax.axis_index(axis) - len(lower)
+    tiles = tiles[(jnp.arange(size) - shift) % size]
+    return joined_along(tiles, dim)
 
 
 def nothing_yet(shard, identity):
@@ -200,9 +222,7 @@
     mixer_result_matrix,
     filter_result_matrix,
 ):
-    normalized_input = row_norm(
-        entry_rescale_vector, lax.all_gather(hidden_activations, "tp", axis=0, tiled=True)
-    )
+    normalized_input = row_norm(entry_rescale_vector, collect(hidden_activations, "tp", 0))
     accumulate = project_rows(normalized_input)
     attn_sums = accumulate(
         empty_slots(normalized_input, (probe_matrix, lookup_address_matrix, payload_matrix)),

time: 312 us -> 296 us (0.949)
  waiting for transfers between devices: 128 us -> 79.4 us
  local copies, waits for them, and re-layouts: 7.15 us -> 27.1 us
  starting transfers between devices: 3.27 us -> 15.1 us
  other arithmetic: 40.2 us -> 44.4 us
    all_gather x2, waiting for transfers between devices: 42.6 us -> 0.02 us  [in_one_piece(): lax.all_gather(both, axis, axis=dim, tiled=True)]
    all_gather x1 -> x0, waiting for transfers between devices: 41.7 us -> none  [body(): lax.all_gather(hidden_activations, 'tp', axis=0, tiled=True)]
    ppermute x0 -> x7, waiting for transfers between devices: none -> 27.7 us  [the longest x4 27.7 us: collect(): lower.append(lax.ppermute(lower[-1] if lower else array, axis, pairs))]
    ppermute x0 -> x7, starting transfers between devices: none -> 13.7 us  [the longest x4 10 us: collect(): lower.append(lax.ppermute(lower[-1] if lower else array, axis, pairs))]
    unnamed x33 -> x32, local copies, waits for them, and re-layouts: 1.87 us -> 12.8 us
    reduce_scatter x1, waiting for transfers between devices: 43 us -> 51.6 us  [body(): lax.psum_scatter((jnp.dot(mixed_attn, mixer_result_matrix, preferred_elem...]
    gather x0 -> x1, local copies, waits for them, and re-layouts: none -> 6.53 us  [collect(): tiles = tiles[(jnp.arange(size) - shift) % size]]
  transfers between devices with their start and end apart: 5 -> 11, of which waited for: 4 -> 5; matrix products, arithmetic and copies ran while one was open for 29% -> 38% of each run, Pallas kernels for 0% -> 0%
where the time goes in v1:
time: 296 us; the launch traced here: 295 us
  waiting for transfers between devices  79.4 us (27%)
  matrix products  72.3 us (24%)
  other arithmetic  44.4 us (15%)
  blocking collectives  43 us (15%)
  local copies, waits for them, and re-layouts  27.1 us (9%)
  starting transfers between devices  15.1 us (5%)
  between operations  13.5 us (5%)
    reduce_scatter x1, waiting for transfers between devices, body(): lax.psum_scatter((jnp.dot(mixed_attn, mixer_result_matrix, preferred_elem...  51.6 us
    all_gather x4, blocking collectives, entering(): lax.all_gather(part.astype(kind), axis)  43 us
    dot_general x5, matrix products, accumulate(): jnp.dot(normalized_input, rows_now, preferred_element_type=jnp.float32)  32.8 us
    ppermute x4, waiting for transfers between devices, collect(): lower.append(lax.ppermute(lower[-1] if lower else array, axis, pairs))  27.7 us
    dot_general x1, matrix products, body(): jnp.dot(mixed_conv, filter_result_matrix, preferred_element_type=jnp.floa...  15.3 us
    add x12, other arithmetic, advance(): return (jnp.exp(decay_now)[..., None] * state + update_now, state)  12.9 us
    unnamed x32, local copies, waits for them, and re-layouts  12.8 us
    ppermute x4, starting transfers between devices, collect(): lower.append(lax.ppermute(lower[-1] if lower else array, axis, pairs))  10 us
  transfers between devices with their start and end apart: 11, of which 5 were waited for; matrix products, arithmetic and copies ran while one was open for 38% of the time, Pallas kernels for 0%

profile of v1, /device:TPU:1, one launch (start us, length us, event | category | flops | bytes accessed | tf_op | source)
XLA Modules:
  0.0 295.0 jit_solution(6194945593022002809)
XLA Ops:
  6.5 1.9 pad_maximum_fusion.2
  8.6 2.6 collective-permute-start
  11.2 9.3 %collective-permute-done = bf16[96,4096]{1,0:T(8,128)(2,1)S(1)} collective-permute-done((bf16[96,4096]{1,0:T(8,128)(2,1)}, bf16[96,4096]{1,0:T(8,128)(2,1)S(1)}, u32[]{:S(2)}, u32[]{:S(2)}) %collective-permute-start) | collective-permute-done | bytes 786464 | tf_op jit(solution)/shard_map/ppermute | solution.py:27
  20.4 2.4 collective-permute-start.1
  22.8 8.9 %collective-permute-done.1 = bf16[96,4096]{1,0:T(8,128)(2,1)} collective-permute-done((bf16[96,4096]{1,0:T(8,128)(2,1)S(1)}, bf16[96,4096]{1,0:T(8,128)(2,1)}, u32[]{:S(2)}, u32[]{:S(2)}) %collective-permute-start.1) | collective-permute-done | bytes 786464 | tf_op jit(solution)/shard_map/ppermute | solution.py:27
  31.7 2.6 collective-permute-start.2
  34.3 2.1 pad_maximum_fusion.1
  36.5 1.2 collective-permute-start.5
  37.7 5.8 %collective-permute-done.2 = bf16[96,4096]{1,0:T(8,128)(2,1)} collective-permute-done((bf16[96,4096]{1,0:T(8,128)(2,1)}, bf16[96,4096]{1,0:T(8,128)(2,1)}, u32[]{:S(2)}, u32[]{:S(2)}) %collective-permute-start.2) | collective-permute-done | bytes 786464 | tf_op jit(solution)/shard_map/ppermute | solution.py:27
  43.6 2.5 collective-permute-start.3
  49.2 2.4 collective-permute-start.6
  51.6 3.7 %collective-permute-done.3 = bf16[96,4096]{1,0:T(8,128)(2,1)} collective-permute-done((bf16[96,4096]{1,0:T(8,128)(2,1)}, bf16[96,4096]{1,0:T(8,128)(2,1)}, u32[]{:S(2)}, u32[]{:S(2)}) %collective-permute-start.3) | collective-permute-done | bytes 786464 | tf_op jit(solution)/shard_map/ppermute | solution.py:27
  55.3 2.1 bitcast_dynamic-update-slice_fusion.8
  57.4 2.1 bitcast_dynamic-update-slice_fusion.7
  59.5 2.1 bitcast_dynamic-update-slice_fusion.6
  64.5 2.1 bitcast_dynamic-update-slice_fusion.2
  67.6 6.5 %gather_fusion = bf16[8,96,4096]{2,1,0:T(8,128)(2,1)} fusion(bf16[8,96,4096]{2,1,0:T(8,128)(2,1)} %bitcast_dynamic-update-slice_fusion.1, s32[1024]{0:T(1024)S(1)} %pad_clamp_fusion), kind=kCustom, calls=%fused_computation | custom fusion | bytes 12582944 | tf_op jit(solution)/shard_map/gather | solution.py:32
  74.1 4.1 %multiply_reduce_fusion = f32[8,96]{1,0:T(8,128)S(1)} fusion(bf16[8,96,4096]{2,1,0:T(8,128)(2,1)} %gather_fusion), kind=kLoop, calls=%fused_computation.9 | loop fusion | flops 9436416 | bytes 6294528 | tf_op jit(solution)/shard_map/reduce_sum | solution.py:80
  78.3 8.2 %fusion.1 = bf16[768,4096]{1,0:T(8,128)(2,1)} fusion(f32[4096]{0:T(1024)S(1)} %convert_element_type.273, f32[768]{0:T(1024)S(1)} %rsqrt.23, bf16[8,96,4096]{2,1,0:T(8,128)(2,1)} %gather_fusion), kind=kLoop, calls=%fused_computation.7 | loop fusion | flops 12582912 | bytes 12602368 | tf_op jit(solution)/shard_map/convert_element_type | solution.py:85
  86.5 5.4 %fusion.50 = f32[768,256]{1,0:T(8,128)S(1)} fusion(bf16[64,256]{1,0:T(8,128)(2,1)S(1)} %copy-done.9, bf16[768,4096]{1,0:T(8,128)(2,1)} %fusion.1, bf16[4096,64]{0,1:T(8,128)(2,1)S(1)} %copy-done, f32[256]{0:T(256)S(1)} %copy-done.10), kind=kOutput, calls=%fused_computation.51 | convolution fusion | flops 429834240 | bytes 7635968 | tf_op jit(solution)/shard_map/dot_general | solution.py:163
  93.1 8.4 %all-gather.2 = bf16[4,2,128]{2,1,0:T(2,128)(2,1)S(1)} all-gather(bf16[1,2,128]{2,1,0:T(2,128)(2,1)S(1)} %fusion.118), channel_id=2, replica_groups=mesh['sp_0'=4,'sp_1'=4,'tp'=8] {'sp_1'}, dimensions={0}, use_global_device_ids=true | all-gather | bytes 2560 | tf_op jit(solution)/shard_map/all_gather | solution.py:48
  101.5 10.5 %all_gather.26 = bf16[4,2,128]{2,1,0:T(2,128)(2,1)S(1)} all-gather(bf16[1,2,128]{2,1,0:T(2,128)(2,1)S(1)} %get-tuple-element.96), channel_id=1, replica_groups=mesh['sp_0'=4,'sp_1'=4,'tp'=8] {'sp_0'}, dimensions={0}, use_global_device_ids=true | all-gather | bytes 2560 | tf_op jit(solution)/shard_map/all_gather | solution.py:48
  112.1 5.2 %fusion.35 = f32[768,256]{1,0:T(8,128)S(1)} fusion(bf16[768,4096]{1,0:T(8,128)(2,1)} %fusion.1, bf16[4096,1024]{1,0:T(8,128)(2,1)} %all-gather.6.cloned.1.call-done), kind=kOutput, calls=%fused_computation.37 | convolution fusion | flops 1611202560 | bytes 9175040 | tf_op jit(solution)/shard_map/dot_general | solution.py:93
  117.7 5.2 %fusion.41 = f32[768,256]{1,0:T(8,128)S(1)} fusion(bf16[768,4096]{1,0:T(8,128)(2,1)} %fusion.1, bf16[4096,1024]{1,0:T(8,128)(2,1)} %all-gather.6.cloned.1.call-done), kind=kOutput, calls=%fused_computation.39 | convolution fusion | flops 1611005952 | bytes 9175040 | tf_op jit(solution)/shard_map/dot_general | solution.py:93
  122.9 1.3 reshape.239
  124.2 7.4 %fusion.14 = bf16[768,512]{1,0:T(8,128)(2,1)S(1)} fusion(bf16[768,4096]{1,0:T(8,128)(2,1)} %fusion.1, bf16[4096,1024]{1,0:T(8,128)(2,1)} %all-gather.6.cloned.1.call-done), kind=kOutput, calls=%fused_computation.28 | convolution fusion | flops 3221618688 | bytes 11272192 | tf_op jit(solution)/shard_map/dot_general | solution.py:93
  131.8 3.9 %copy_multiply_fusion = (f32[12,64,2,128]{3,0,1,2:T(8,128)S(1)}, f32[12,64,2,128]{3,0,1,2:T(8,128)}, f32[12,64,2,128]{3,0,1,2:T(8,128)}, f32[12,64,2,128]{3,0,1,2:T(8,128)S(1)}) fusion(f32[12,64,2,128]{3,2,1,0:T(2,128)} %reshape.239, f32[12,64,2,128]{3,0,1,2:T(8,128)} %copy-done.4, f32[12,2,128]{2,0,1:T(8,128)S(1)} %get-tuple-element.140, ...), kind=kLoop, calls=%fused_computation.41 | loop fusion | flops 1179648 | bytes 5529600 | tf_op jit(solution)/shard_map/mul | solution.py:122
  135.7 3.2 %fusion.52 = f32[12,2,128,256]{3,2,1,0:T(8,128)} fusion(f32[12,64,2,128]{3,0,1,2:T(8,128)S(1)} %get-tuple-element.85, bf16[12,64,2,256]{3,2,1,0:T(2,128)(2,1)S(1)} %reshape.235), kind=kOutput, calls=%fused_computation.63 | convolution fusion | flops 603979776 | bytes 4718592 | tf_op jit(solution)/shard_map/njhd,njhv->nhdv/dot_general | solution.py:128
  138.8 22.1 %while.13 = (s32[]{:T(128)}, f32[2,128,256]{2,1,0:T(8,128)S(1)}, f32[12,2,128,256]{3,2,1,0:T(8,128)}, f32[12,2,128]{2,0,1:T(8,128)S(1)}, f32[12,2,128,256]{3,2,1,0:T(8,128)}, /*index=5*/s32[]{:T(128)}, s32[]{:T(128)}) while((s32[]{:T(128)}, f32[2,128,256]{2,1,0:T(8,128)S(1)}, f32[12,2,128,256]{3,2,1,0:T(8,128)}, ...), condition=%wide.region_3.4_spmd.clone, body=%wide.region_2.3_spmd.clone.sunk | while | flops 262147 | bytes 1316448 | solution.py:135
  141.4 1.1 bitcast_add_fusion.3
  143.3 1.1 bitcast_add_fusion.3
  146.9 1.1 bitcast_add_fusion.3
  150.6 1.1 bitcast_add_fusion.3
  159.9 1.1 bitcast_add_fusion.3
  161.0 13.7 %all-gather.1 = bf16[8,128,256]{2,1,0:T(8,128)(2,1)S(1)} all-gather(bf16[2,128,256]{2,1,0:T(8,128)(2,1)S(1)} %convert_element_type.304), channel_id=3, replica_groups=mesh['sp_0'=4,'sp_1'=4,'tp'=8] {'sp_1'}, dimensions={0}, use_global_device_ids=true | all-gather | bytes 655360 | tf_op jit(solution)/shard_map/all_gather | solution.py:48
  174.9 10.4 %all_gather.29 = bf16[4,2,128,256]{3,2,1,0:T(8,128)(2,1)S(1)} all-gather(bf16[1,2,128,256]{3,2,1,0:T(8,128)(2,1)S(1)} %fusion.78), channel_id=1, replica_groups=mesh['sp_0'=4,'sp_1'=4,'tp'=8] {'sp_0'}, dimensions={0}, use_global_device_ids=true | all-gather | bytes 655360 | tf_op jit(solution)/shard_map/all_gather | solution.py:48
  185.3 3.0 %convolution_select_fusion = f32[12,2,64,64]{3,2,1,0:T(8,128)S(1)} fusion(f32[12,64,2,128]{3,0,1,2:T(8,128)} %get-tuple-element.86, f32[12,64,2,128]{3,0,1,2:T(8,128)S(1)} %get-tuple-element.91, pred[64,64]{1,0:T(8,128)(4,1)S(1)} %iota_compare_fusion), kind=kOutput, calls=%fused_computation.32 | convolution fusion | flops 151093248 | bytes 1970176 | tf_op jit(solution)/shard_map/nihd,njhd->nhij/dot_general | solution.py:124
  189.2 2.1 fusion.59
  191.3 3.4 %multiply_reduce_fusion.1 = (f32[12,64,2]{1,2,0:T(2,128)S(1)}, f32[12,64,2,256]{3,1,2,0:T(8,128)}) fusion(f32[12,64,2,128]{3,0,1,2:T(8,128)S(1)} %copy-done.6, bf16[4,2,128,256]{3,2,1,0:T(8,128)(2,1)S(1)} %all_gather.29, f32[2,128]{1,0:T(2,128)S(1)} %get-tuple-element.97, f32[2,128]{1,0:T(2,128)S(1)} %get-tuple-element.103, ...), kind=kOutput, calls=%fused_computation.27 | convolution fusion | flops 607648256 | bytes 6568968 | tf_op jit(solution)/shard_map/nihd,hdv->nihv/dot_general | solution.py:178
  194.9 1.2 mul.291
  196.3 1.2 copy.69
  197.5 1.3 copy.75
  198.8 7.4 %fusion.17 = bf16[768,512]{1,0:T(8,128)(2,1)S(1)} fusion(bf16[768,4096]{1,0:T(8,128)(2,1)} %fusion.1, bf16[4096,1536]{1,0:T(8,128)(2,1)} %all-gather.8.cloned.1.call-done), kind=kOutput, calls=%fused_computation.29 | convolution fusion | flops 3221618688 | bytes 11272192 | tf_op jit(solution)/shard_map/dot_general | solution.py:93
  206.3 7.6 %multiply_convert_fusion.1 = bf16[768,512]{1,0:T(8,128)(2,1)S(1)} fusion(bf16[768,512]{1,0:T(8,128)(2,1)S(1)} %fusion.17, bf16[768,4096]{1,0:T(8,128)(2,1)} %fusion.1, bf16[4096,1536]{1,0:T(8,128)(2,1)} %all-gather.8.cloned.1.call-done), kind=kOutput, calls=%fused_computation.25 | convolution fusion | flops 3223191552 | bytes 12058624 | tf_op jit(solution)/shard_map/dot_general | solution.py:93
  213.8 1.3 collective-permute-start.7
  215.2 6.4 %fusion.48 = f32[768,4096]{1,0:T(8,128)} fusion(bf16[512,4096]{1,0:T(8,128)(2,1)S(1)} %copy-done.5, f32[768,512]{1,0:T(8,128)S(1)} %bitcast.205, f32[768,512]{1,0:T(8,128)S(1)} %bitcast.204, f32[512]{0:T(512)S(1)} %bitcast.210), kind=kOutput, calls=%fused_computation.49 | convolution fusion | flops 3222405120 | bytes 19924992 | tf_op jit(solution)/shard_map/dot_general | solution.py:254
  221.6 15.3 %add_convert_fusion = bf16[768,4096]{1,0:T(8,128)(2,1)} fusion(f32[768,4096]{1,0:T(8,128)} %fusion.48, bf16[512,4096]{1,0:T(8,128)(2,1)} %param.33, bf16[768,512]{1,0:T(8,128)(2,1)S(1)} %multiply_convert_fusion.1, bf16[768,4096]{1,0:T(8,128)(2,1)} %fusion.1, bf16[4096,1536]{1,0:T(8,128)(2,1)} %all-gather.8.cloned.1.call-done, ...), kind=kOutput, calls=%fused_computation.8 | convolution fusion | flops 6455820288 | bytes 34349056 | tf_op jit(solution)/shard_map/dot_general | solution.py:255
  236.9 51.6 %reduce-scatter.2.cloned.1.call-done = bf16[96,4096]{1,0:T(8,128)(2,1)} async-done(((bf16[768,4096]{1,0:T(8,128)(2,1)}), bf16[96,4096]{1,0:T(8,128)(2,1)}) %reduce-scatter.2.cloned.1.call-update) | async-done | bytes 786448 | tf_op jit(solution)/shard_map/reduce_scatter | solution.py:252
  (114 shorter events, 26.9 us)
Async XLA Ops:
  6.5 80.0 %copy-start = (bf16[4096,64]{0,1:T(8,128)(2,1)S(1)}, bf16[4096,64]{0,1:T(8,128)(2,1)}, u32[]{:S(2)}) copy-start(bf16[4096,64]{0,1:T(8,128)(2,1)} %param.26) | copy-start | bytes 1572868
  6.5 105.5 %all-gather.6.cloned.1.call-start = ((), (), s32[]{:S(2)}) async-start(), calls=%async_computation.1 | async-start | bytes 8912896 | tf_op jit(solution)/shard_map/all_gather | solution.py:71
  8.5 54.0 %copy-start.8 = (bf16[96,4096]{1,0:T(8,128)(2,1)S(1)}, bf16[96,4096]{1,0:T(8,128)(2,1)}, u32[]{:S(2)}) copy-start(bf16[96,4096]{1,0:T(8,128)(2,1)} %param.18) | copy-start | bytes 2359300
  8.5 190.3 %all-gather.8.cloned.1.call-start = ((), (), s32[]{:S(2)}) async-start(), calls=%async_computation.2 | async-start | bytes 13369344 | tf_op jit(solution)/shard_map/all_gather | solution.py:71
  8.6 11.9 %collective-permute-start = (bf16[96,4096]{1,0:T(8,128)(2,1)}, bf16[96,4096]{1,0:T(8,128)(2,1)S(1)}, u32[]{:S(2)}, u32[]{:S(2)}) collective-permute-start(bf16[96,4096]{1,0:T(8,128)(2,1)} %param.18), channel_id=1, source_target_pairs={{0,1},{1,2},{2,3},{3,4},{4,5},{5,6},{6,7},{7,0},{8,9},{9,10},{10,1... | collective-permute-start | bytes 2359304 | tf_op jit(solution)/shard_map/ppermute | solution.py:27
  20.4 11.3 %collective-permute-start.1 = (bf16[96,4096]{1,0:T(8,128)(2,1)S(1)}, bf16[96,4096]{1,0:T(8,128)(2,1)}, u32[]{:S(2)}, u32[]{:S(2)}) collective-permute-start(bf16[96,4096]{1,0:T(8,128)(2,1)S(1)} %collective-permute-done), channel_id=1, source_target_pairs={{0,1},{1,2},{2,3},{3,4},{4,5},{5,6},{6,7},{7,0},{8,9},{9,10},{10,1... | collective-permute-start | bytes 2359304 | tf_op jit(solution)/shard_map/ppermute | solution.py:27
  22.8 13.7 %collective-permute-start.4 = (bf16[96,4096]{1,0:T(8,128)(2,1)}, bf16[96,4096]{1,0:T(8,128)(2,1)S(1)}, u32[]{:S(2)}, u32[]{:S(2)}) collective-permute-start(bf16[96,4096]{1,0:T(8,128)(2,1)} %param.18), channel_id=1, source_target_pairs={{1,0},{2,1},{3,2},{4,3},{5,4},{6,5},{7,6},{0,7},{9,8},{10,9},{11,1... | collective-permute-start | bytes 2359304 | tf_op jit(solution)/shard_map/ppermute | solution.py:29
  31.7 11.8 %collective-permute-start.2 = (bf16[96,4096]{1,0:T(8,128)(2,1)}, bf16[96,4096]{1,0:T(8,128)(2,1)}, u32[]{:S(2)}, u32[]{:S(2)}) collective-permute-start(bf16[96,4096]{1,0:T(8,128)(2,1)} %collective-permute-done.1), channel_id=1, source_target_pairs={{0,1},{1,2},{2,3},{3,4},{4,5},{5,6},{6,7},{7,0},{8,9},{9,10},{10,1... | collective-permute-start | bytes 2359304 | tf_op jit(solution)/shard_map/ppermute | solution.py:27
  36.4 252.0 %reduce-scatter.2.cloned.1.call-start = ((), (), s32[]{:S(2)}) async-start(), calls=%async_computation.3 | async-start | bytes 7077888 | tf_op jit(solution)/shard_map/reduce_scatter | solution.py:252
  36.5 12.7 %collective-permute-start.5 = (bf16[96,4096]{1,0:T(8,128)(2,1)S(1)}, bf16[96,4096]{1,0:T(8,128)(2,1)}, u32[]{:S(2)}, u32[]{:S(2)}) collective-permute-start(bf16[96,4096]{1,0:T(8,128)(2,1)S(1)} %collective-permute-done.4), channel_id=1, source_target_pairs={{1,0},{2,1},{3,2},{4,3},{5,4},{6,5},{7,6},{0,7},{9,8},{10,9},{11,1... | collective-permute-start | bytes 2359304 | tf_op jit(solution)/shard_map/ppermute | solution.py:29
  43.6 11.7 %collective-permute-start.3 = (bf16[96,4096]{1,0:T(8,128)(2,1)}, bf16[96,4096]{1,0:T(8,128)(2,1)}, u32[]{:S(2)}, u32[]{:S(2)}) collective-permute-start(bf16[96,4096]{1,0:T(8,128)(2,1)} %collective-permute-done.2), channel_id=1, source_target_pairs={{0,1},{1,2},{2,3},{3,4},{4,5},{5,6},{6,7},{7,0},{8,9},{9,10},{10,1... | collective-permute-start | bytes 2359304 | tf_op jit(solution)/shard_map/ppermute | solution.py:27
  49.2 17.4 %collective-permute-start.6 = (bf16[96,4096]{1,0:T(8,128)(2,1)}, bf16[96,4096]{1,0:T(8,128)(2,1)S(1)}, u32[]{:S(2)}, u32[]{:S(2)}) collective-permute-start(bf16[96,4096]{1,0:T(8,128)(2,1)} %collective-permute-done.5), channel_id=1, source_target_pairs={{1,0},{2,1},{3,2},{4,3},{5,4},{6,5},{7,6},{0,7},{9,8},{10,9},{11,1... | collective-permute-start | bytes 2359304 | tf_op jit(solution)/shard_map/ppermute | solution.py:29
  78.3 8.2 %copy-start.9 = (bf16[64,256]{1,0:T(8,128)(2,1)S(1)}, bf16[64,256]{1,0:T(8,128)(2,1)}, u32[]{:S(2)}) copy-start(bf16[64,256]{1,0:T(8,128)(2,1)} %param.27) | copy-start | bytes 98308
  78.3 8.2 %copy-start.10 = (f32[256]{0:T(256)S(1)}, f32[256]{0:T(256)}, u32[]{:S(2)}) copy-start(f32[256]{0:T(256)} %param.28) | copy-start | bytes 3076
  93.0 24.2 %copy-start.4 = (f32[12,64,2,128]{3,0,1,2:T(8,128)}, f32[12,64,2,128]{3,0,1,2:T(8,128)S(1)}, u32[]{:S(2)}) copy-start(f32[12,64,2,128]{3,0,1,2:T(8,128)S(1)} %fusion.46) | copy-start | bytes 2359300
  161.0 28.2 %copy-start.7 = (f32[12,2,128,256]{3,2,1,0:T(8,128)S(1)}, f32[12,2,128,256]{3,2,1,0:T(8,128)}, u32[]{:S(2)}) copy-start(f32[12,2,128,256]{3,2,1,0:T(8,128)} %get-tuple-element.33) | copy-start | bytes 9437188
  188.4 2.9 copy-start.6
  194.9 1.4 copy-start.3
  206.2 8.9 %copy-start.2 = (f32[96,8,2,256]{3,1,2,0:T(8,128)S(1)}, f32[96,8,2,256]{3,1,2,0:T(8,128)}, u32[]{:S(2)}) copy-start(f32[96,8,2,256]{3,1,2,0:T(8,128)} %copy.75) | copy-start | bytes 4718596
  206.3 8.9 %copy-start.5 = (bf16[512,4096]{1,0:T(8,128)(2,1)S(1)}, bf16[512,4096]{1,0:T(8,128)(2,1)}, u32[]{:S(2)}) copy-start(bf16[512,4096]{1,0:T(8,128)(2,1)} %param.32) | copy-start | bytes 12582916
  213.8 7.7 %collective-permute-start.7 = (bf16[2,512]{1,0:T(2,128)(2,1)S(1)}, bf16[2,512]{1,0:T(2,128)(2,1)S(1)}, u32[]{:S(2)}, u32[]{:S(2)}) collective-permute-start(bf16[2,512]{1,0:T(2,128)(2,1)S(1)} %slice.153), channel_id=1, source_target_pairs={{0,8},{8,16},{16,24},{24,32},{32,40},{40,48},{48,56},{56,64},{64,7... | collective-permute-start | bytes 6152 | tf_op jit(solution)/shard_map/ppermute | solution.py:66
  221.6 66.9 %copy-start.1 = (bf16[4096,64]{0,1:T(8,128)(2,1)S(1)}, bf16[4096,64]{0,1:T(8,128)(2,1)}, u32[]{:S(2)}) copy-start(bf16[4096,64]{0,1:T(8,128)(2,1)} %param.26) | copy-start | bytes 1572868
Sparse Core Ops, SparseCore 0:
  9.5 73.9 all-gather.5
  85.6 91.4 all-gather.7
  237.0 51.3 reduce-scatter.1
